TPU v7x, 32 devices: a whole 2x2x4 slice. The times are simulated.
32 devices in a mesh: ep: 8 (over z, core), tp: 4 (over y, x).
Axes of the slice: x: 2, y: 2, z: 4, core: 2. Of those that a mesh axis runs over, the one named last changes fastest.
Arguments:
- tokens: bfloat16 [1024, 2048], P('ep'), may hold values from -6 to 6
- chosen: int32 [8, 8, 8], replicated, may hold values from 0 to 127, as said below
- chosen_weight: float32 [8, 8, 8], P('ep'), may hold values from 0.1 to 1
- gate_weight: bfloat16 [8, 2048, 4096], P('ep', None, 'tp'), may hold values from -0.125 to 0.125
- up_weight: bfloat16 [8, 2048, 4096], P('ep', None, 'tp'), may hold values from -0.125 to 0.125
- down_weight: bfloat16 [8, 4096, 2048], P('ep', 'tp'), may hold values from -0.09375 to 0.09375
Outputs:
- combined: bfloat16 [1024, 2048], P('ep', 'tp')
Inputs may be any that keep to these rules, and one draw needn't show every extreme that they name: `chosen`: for every block and expert the 8 positions are distinct.
All inputs are finite; a program needn't handle non-finite values.
Results may differ from a plain program's by a relative error of at most 0.015.
Values may be sent and summed in bfloat16 or wider, within the bound.
A program may use at most 64 MiB of HBM per device.

v0:
```python
import jax
import jax.numpy as jnp
from jax import lax
from jax.sharding import PartitionSpec as P


def local(tokens, chosen, chosen_weight, gate_weight, up_weight, down_weight):
    ep_index = lax.axis_index("ep")
    tp_count = lax.axis_size("tp")
    tp_index = lax.axis_index("tp")
    tok_count, model_width = tokens.shape
    blocks, experts, picks_each = chosen.shape
    slice_width = model_width // tp_count
    columns = lax.dynamic_slice_in_dim(tokens, tp_index * slice_width, slice_width, 1)
    outgoing = lax.dynamic_index_in_dim(chosen, ep_index, 0, keepdims=False)
    leaving = jnp.take(columns, outgoing.reshape(-1), axis=0).reshape(
        experts, picks_each, slice_width
    )
    arrived = lax.all_to_all(leaving, "ep", split_axis=0, concat_axis=0, tiled=True).reshape(
        blocks * picks_each, slice_width
    )
    gate_local = gate_weight[0]
    up_local = up_weight[0]
    portion = lax.all_gather(arrived, "tp", axis=1, tiled=True)
    gate_sum = jnp.dot(portion, gate_local, preferred_element_type=jnp.float32)
    up_sum = jnp.dot(portion, up_local, preferred_element_type=jnp.float32)
    hidden = (jax.nn.silu(gate_sum) * up_sum).astype(jnp.bfloat16)
    down_local = down_weight[0].reshape(down_weight.shape[1], tp_count, slice_width)
    summed = lax.psum_scatter(
        jnp.einsum("rf,fcd->crd", hidden, down_local, preferred_element_type=jnp.float32).astype(
            jnp.bfloat16
        ),
        "tp",
        scatter_dimension=0,
        tiled=True,
    ).astype(jnp.float32)
    expert_out = summed[0].astype(jnp.bfloat16).reshape(blocks, picks_each, slice_width)
    returned = lax.all_to_all(expert_out, "ep", split_axis=0, concat_axis=0, tiled=True).reshape(
        experts * picks_each, slice_width
    )
    positions = jnp.arange(tok_count, dtype=jnp.int32)[:, None]
    placement_matrix = jnp.where(
        outgoing.reshape(1, -1) == positions, chosen_weight[0].reshape(1, -1), 0.0
    )
    combined = jnp.dot(
        placement_matrix,
        returned.astype(jnp.float32),
        precision=lax.Precision.HIGHEST,
        preferred_element_type=jnp.float32,
    )
    return combined.astype(jnp.bfloat16)


def solution(mesh):
    return jax.shard_map(
        local,
        mesh=mesh,
        in_specs=(
            P("ep", None),
            P(),
            P("ep", None, None),
            P("ep", None, "tp"),
            P("ep", None, "tp"),
            P("ep", "tp", None),
        ),
        out_specs=P("ep", "tp"),
        check_vma=False,
    )
```

profile of v0, /device:TPU:0, one launch (start us, length us, event | category | flops | bytes accessed | tf_op | source)
XLA Modules:
  0.0 84.8 jit_solution(2384732761228838541)
XLA Ops:
  6.5 0.0 copy-start
  6.5 0.8 compare_and_fusion
  7.3 0.1 reshape.58
  7.4 0.2 copy-done
  7.6 0.7 gather_fusion
  8.3 0.7 bitcast_select_fusion
  9.0 6.4 %all-to-all-start = ((bf16[8,8,512]{2,1,0:T(8,128)(2,1)}), bf16[8,8,512]{2,1,0:T(8,128)(2,1)S(1)}, u32[]{:S(2)}, u32[]{:S(2)}) async-start(bf16[8,8,512]{2,1,0:T(8,128)(2,1)} %bitcast_select_fusion), calls=%async_computation | async-start | bytes 131072 | tf_op jit(solution)/shard_map/all_to_all | solution.py:19
  15.4 0.0 reduce-scatter.4.cloned.1.call-start
  15.4 7.8 %reshape_squeeze.4 = bf16[1024,4,512]{2,1,0:T(4,128)(2,1)} reshape(bf16[1,1024,2048]{2,1,0:T(8,128)(2,1)} %param.11) | data formatting | bytes 8388608 | tf_op jit(solution)/shard_map/reshape;squeeze | solution.py:28
  23.2 0.0 all-to-all-done
  23.2 9.0 %all_gather.3 = bf16[64,2048]{1,0:T(8,128)(2,1)S(1)} all-gather(bf16[64,512]{1,0:T(8,128)(2,1)S(1)} %bitcast.36), channel_id=1, replica_groups=mesh['ep'=8,'tp'=4] {'tp'}, dimensions={1}, use_global_device_ids=true | all-gather | bytes 327680 | tf_op jit(solution)/shard_map/all_gather | solution.py:24
  32.2 3.0 %fusion.2 = f32[64,1024]{1,0:T(8,128)S(1)} fusion(bf16[64,2048]{1,0:T(8,128)(2,1)S(1)} %all_gather.3, bf16[1,2048,1024]{2,1,0:T(8,128)(2,1)} %param.9), kind=kOutput, calls=%fused_computation.3 | convolution fusion | flops 268435456 | bytes 4718592 | tf_op jit(solution)/shard_map/dot_general | solution.py:25
  35.2 0.0 copy-start.1
  35.2 6.3 %fusion.12 = bf16[4,64,512]{2,1,0:T(8,128)(2,1)} fusion(bf16[1024,4,512]{2,1,0:T(4,128)(2,1)} %reshape_squeeze.4, bf16[64,2048]{1,0:T(8,128)(2,1)S(1)} %all_gather.3, bf16[1,2048,1024]{2,1,0:T(8,128)(2,1)} %param.10, f32[64,1024]{1,0:T(8,128)S(1)} %fusion.2), kind=kOutput, calls=%fused_computation.9 | convolution fusion | flops 537395200 | bytes 9175040 | tf_op jit(solution)/shard_map/rf,fcd->crd/dot_general | solution.py:30
  41.6 0.0 reduce-scatter.4.cloned.1.call-update
  41.6 25.0 %reduce-scatter.4.cloned.1.call-done = bf16[1,64,512]{2,1,0:T(8,128)(2,1)} async-done(((bf16[4,64,512]{2,1,0:T(8,128)(2,1)}), bf16[1,64,512]{2,1,0:T(8,128)(2,1)}) %reduce-scatter.4.cloned.1.call-update) | async-done | bytes 65552
  66.6 4.6 %all-to-all-start.1 = ((bf16[8,8,512]{2,1,0:T(8,128)(2,1)}), bf16[8,8,512]{2,1,0:T(8,128)(2,1)S(1)}, u32[]{:S(2)}, u32[]{:S(2)}) async-start(bf16[8,8,512]{2,1,0:T(8,128)(2,1)} %bitcast.37), calls=%async_computation.1 | async-start | bytes 131072 | tf_op jit(solution)/shard_map/all_to_all | solution.py:38
  71.2 0.1 eq.17
  71.3 0.0 copy-done.1
  71.3 0.1 broadcast_in_dim.25
  71.3 5.8 %all-to-all-done.1 = bf16[8,8,512]{2,1,0:T(8,128)(2,1)S(1)} async-done(((bf16[8,8,512]{2,1,0:T(8,128)(2,1)}), bf16[8,8,512]{2,1,0:T(8,128)(2,1)S(1)}, u32[]{:S(2)}, u32[]{:S(2)}) %all-to-all-start.1) | async-done | bytes 65568 | tf_op jit(solution)/shard_map/all_to_all | solution.py:38
  77.1 0.9 %convolution_convert_fusion = bf16[128,512]{1,0:T(8,128)(2,1)} fusion(bf16[8,8,512]{2,1,0:T(8,128)(2,1)S(1)} %all-to-all-done.1, f32[64]{0:T(128)S(1)} %broadcast_in_dim.25, s32[64]{0:T(128)S(1)} %eq.17), kind=kOutput, calls=%fused_computation.11 | convolution fusion | flops 50413568 | bytes 197120 | tf_op jit(solution)/shard_map/dot_general | solution.py:45
  (3 shorter events, 0.0 us)
Async XLA Ops:
  6.5 1.1 %copy-start = (bf16[128,2048]{1,0:T(8,128)(2,1)S(1)}, bf16[128,2048]{1,0:T(8,128)(2,1)}, u32[]{:S(2)}) copy-start(bf16[128,2048]{1,0:T(8,128)(2,1)} %param.6) | copy-start | bytes 1572868
  9.0 14.2 %all-to-all-start = ((bf16[8,8,512]{2,1,0:T(8,128)(2,1)}), bf16[8,8,512]{2,1,0:T(8,128)(2,1)S(1)}, u32[]{:S(2)}, u32[]{:S(2)}) async-start(bf16[8,8,512]{2,1,0:T(8,128)(2,1)} %bitcast_select_fusion), calls=%async_computation | async-start | bytes 131072 | tf_op jit(solution)/shard_map/all_to_all | solution.py:19
  15.4 51.2 %reduce-scatter.4.cloned.1.call-start = ((), (), s32[]{:S(2)}) async-start(), calls=%async_computation.3 | async-start | bytes 327680
  35.2 36.0 %copy-start.1 = (f32[1,8,8]{2,1,0:T(8,128)S(1)}, f32[1,8,8]{2,1,0:T(8,128)}, u32[]{:S(2)}) copy-start(f32[1,8,8]{2,1,0:T(8,128)} %param.8) | copy-start | bytes 772
  66.6 10.5 %all-to-all-start.1 = ((bf16[8,8,512]{2,1,0:T(8,128)(2,1)}), bf16[8,8,512]{2,1,0:T(8,128)(2,1)S(1)}, u32[]{:S(2)}, u32[]{:S(2)}) async-start(bf16[8,8,512]{2,1,0:T(8,128)(2,1)} %bitcast.37), calls=%async_computation.1 | async-start | bytes 131072 | tf_op jit(solution)/shard_map/all_to_all | solution.py:38
Sparse Core Ops, SparseCore 0:
  41.7 24.7 reduce-scatter.3
where the time goes:
time: 85.3 us; the launch traced here: 84.8 us
  waiting for transfers between devices  30.7 us (36%)
  between operations  13.4 us (16%)
  starting transfers between devices  11 us (13%)
  matrix products  10.3 us (12%)
  blocking collectives  8.98 us (11%)
  local copies, waits for them, and re-layouts  8.96 us (11%)
  other arithmetic  1.48 us (2%)
    unnamed x2, waiting for transfers between devices  25 us
    all_gather x1, blocking collectives, local(): portion = lax.all_gather(arrived, 'tp', axis=1, tiled=True)  8.98 us
    another operation x1, local copies, waits for them, and re-layouts, local(): down_weight[0].reshape(down_weight.shape[1], tp_count, slice_width)  7.8 us
    all_to_all x1, starting transfers between devices, local(): lax.all_to_all(leaving, 'ep', split_axis=0, concat_axis=0, tiled=True)  6.35 us
    dot_general x1, matrix products, local(): jnp.einsum('rf,fcd->crd', hidden, down_local, preferred_element_type=jnp....  6.33 us
    all_to_all x1, waiting for transfers between devices, local(): lax.all_to_all(expert_out, 'ep', split_axis=0, concat_axis=0, tiled=True)  5.76 us
    all_to_all x1, starting transfers between devices, local(): lax.all_to_all(expert_out, 'ep', split_axis=0, concat_axis=0, tiled=True)  4.61 us
    dot_general x1, matrix products, local(): gate_sum = jnp.dot(portion, gate_local, preferred_element_type=jnp.float32)  3.03 us
  transfers between devices with their start and end apart: 3, of which 2 were waited for; matrix products, arithmetic and copies ran while one was open for 9% of the time, Pallas kernels for 0%

commit v1 on v0

--- a/solution.py
+++ b/solution.py
@@ -2,6 +2,29 @@
 import jax.numpy as jnp
 from jax import lax
 from jax.sharding import PartitionSpec as P
+
+
+def in_blocks(x, dim, size):
+    dims = x.shape
+    parts = x.reshape(*dims[:dim], size, dims[dim] // size, *dims[dim + 1 :])
+    return jnp.moveaxis(parts, dim, 0)
+
+
+def laid_out(blocks, dim):
+    lengths = list(blocks.shape[1:])
+    lengths[dim] *= blocks.shape[0]
+    return jnp.moveaxis(blocks, 0, dim).reshape(lengths)
+
+
+def exchange_directly(x, axis, split_dim, concat_dim):
+    size, place = (lax.axis_size(axis), lax.axis_index(axis))
+    blocks = in_blocks(x, split_dim, size)
+    outs = [blocks[place]]
+    for step in range(1, size):
+        sent = blocks[(place + step) % size]
+        outs.append(lax.ppermute(sent, axis, [(i, (i + step) % size) for i in range(size)]))
+    blocks = jnp.stack(outs)[(place - jnp.arange(size)) % size]
+    return laid_out(blocks, concat_dim)
 
 
 def local(tokens, chosen, chosen_weight, gate_weight, up_weight, down_weight):
@@ -16,9 +39,7 @@
     leaving = jnp.take(columns, outgoing.reshape(-1), axis=0).reshape(
         experts, picks_each, slice_width
     )
-    arrived = lax.all_to_all(leaving, "ep", split_axis=0, concat_axis=0, tiled=True).reshape(
-        blocks * picks_each, slice_width
-    )
+    arrived = exchange_directly(leaving, "ep", 0, 0).reshape(blocks * picks_each, slice_width)
     gate_local = gate_weight[0]
     up_local = up_weight[0]
     portion = lax.all_gather(arrived, "tp", axis=1, tiled=True)

time: 85.3 us -> 93.1 us (1.091)
  waiting for transfers between devices: 30.7 us -> 36.9 us
  starting transfers between devices: 11 us -> 12.5 us
    ppermute x0 -> x7, waiting for transfers between devices: none -> 9.42 us  [exchange_directly(): lax.ppermute(sent, axis, [(i, (i + step) % size) for i in range(size)])]
    ppermute x0 -> x7, starting transfers between devices: none -> 7.9 us  [exchange_directly(): lax.ppermute(sent, axis, [(i, (i + step) % size) for i in range(size)])]
    all_to_all x1 -> x0, starting transfers between devices: 6.35 us -> none  [local(): lax.all_to_all(leaving, 'ep', split_axis=0, concat_axis=0, tiled=True)]
    unnamed x2, waiting for transfers between devices: 25 us -> 21.8 us
  transfers between devices with their start and end apart: 3 -> 9, of which waited for: 2 -> 4; matrix products, arithmetic and copies ran while one was open for 9% -> 9% of each run, Pallas kernels for 0% -> 0%
where the time goes in v1:
time: 93.1 us; the launch traced here: 92.6 us
  waiting for transfers between devices  36.9 us (40%)
  between operations  13.5 us (15%)
  starting transfers between devices  12.5 us (13%)
  matrix products  10.3 us (11%)
  local copies, waits for them, and re-layouts  9.52 us (10%)
  blocking collectives  8.99 us (10%)
    unnamed x2, waiting for transfers between devices  21.8 us
    ppermute x7, waiting for transfers between devices, exchange_directly(): lax.ppermute(sent, axis, [(i, (i + step) % size) for i in range(size)])  9.42 us
    all_gather x1, blocking collectives, local(): portion = lax.all_gather(arrived, 'tp', axis=1, tiled=True)  8.99 us
    ppermute x7, starting transfers between devices, exchange_directly(): lax.ppermute(sent, axis, [(i, (i + step) % size) for i in range(size)])  7.9 us
    another operation x1, local copies, waits for them, and re-layouts, local(): down_weight[0].reshape(down_weight.shape[1], tp_count, slice_width)  7.81 us
    dot_general x1, matrix products, local(): jnp.einsum('rf,fcd->crd', hidden, down_local, preferred_element_type=jnp....  6.33 us
    all_to_all x1, waiting for transfers between devices, local(): lax.all_to_all(expert_out, 'ep', split_axis=0, concat_axis=0, tiled=True)  5.76 us
    all_to_all x1, starting transfers between devices, local(): lax.all_to_all(expert_out, 'ep', split_axis=0, concat_axis=0, tiled=True)  4.62 us
  transfers between devices with their start and end apart: 9, of which 4 were waited for; matrix products, arithmetic and copies ran while one was open for 9% of the time, Pallas kernels for 0%

profile of v1, /device:TPU:0, one launch (start us, length us, event | category | flops | bytes accessed | tf_op | source)
XLA Modules:
  0.0 92.6 jit_solution(522080417674637723)
XLA Ops:
  6.5 0.8 compare_and_fusion
  7.3 0.1 reshape.114
  7.4 0.2 copy-done
  7.6 0.7 gather_fusion
  8.3 0.1 bitcast_select_fusion
  8.4 4.6 %collective-permute-start.6 = (bf16[1,8,512]{2,1,0:T(8,128)(2,1)S(1)}, bf16[1,8,512]{2,1,0:T(8,128)(2,1)S(1)}, u32[]{:S(2)}, u32[]{:S(2)}) collective-permute-start(bf16[1,8,512]{2,1,0:T(8,128)(2,1)S(1)} %get-tuple-element.7), channel_id=1, source_target_pairs={{0,28},{4,0},{8,4},{12,8},{16,12},{20,16},{24,20},{28,24},{1,29},{... | collective-permute-start | bytes 24584 | tf_op jit(solution)/shard_map/ppermute | solution.py:25
  13.0 0.6 collective-permute-start.5
  13.6 2.7 %collective-permute-start.3 = (bf16[1,8,512]{2,1,0:T(8,128)(2,1)S(1)}, bf16[1,8,512]{2,1,0:T(8,128)(2,1)S(1)}, u32[]{:S(2)}, u32[]{:S(2)}) collective-permute-start(bf16[1,8,512]{2,1,0:T(8,128)(2,1)S(1)} %get-tuple-element.10), channel_id=1, source_target_pairs={{0,16},{4,20},{8,24},{12,28},{16,0},{20,4},{24,8},{28,12},{1,17},{... | collective-permute-start | bytes 24584 | tf_op jit(solution)/shard_map/ppermute | solution.py:25
  16.3 0.0 collective-permute-start
  16.3 7.8 %reshape_squeeze.4 = bf16[1024,4,512]{2,1,0:T(4,128)(2,1)} reshape(bf16[1,1024,2048]{2,1,0:T(8,128)(2,1)} %param.11) | data formatting | bytes 8388608 | tf_op jit(solution)/shard_map/reshape;squeeze | solution.py:49
  24.2 5.4 %collective-permute-done.1 = bf16[1,8,512]{2,1,0:T(8,128)(2,1)S(1)} collective-permute-done((bf16[1,8,512]{2,1,0:T(8,128)(2,1)S(1)}, bf16[1,8,512]{2,1,0:T(8,128)(2,1)S(1)}, u32[]{:S(2)}, u32[]{:S(2)}) %collective-permute-start.1) | collective-permute-done | bytes 8224 | tf_op jit(solution)/shard_map/ppermute | solution.py:25
  29.6 4.0 %collective-permute-done.2 = bf16[1,8,512]{2,1,0:T(8,128)(2,1)S(1)} collective-permute-done((bf16[1,8,512]{2,1,0:T(8,128)(2,1)S(1)}, bf16[1,8,512]{2,1,0:T(8,128)(2,1)S(1)}, u32[]{:S(2)}, u32[]{:S(2)}) %collective-permute-start.2) | collective-permute-done | bytes 8224 | tf_op jit(solution)/shard_map/ppermute | solution.py:25
  33.7 0.6 gather_fusion.1
  34.2 9.0 %all_gather.3 = bf16[64,2048]{1,0:T(8,128)(2,1)S(1)} all-gather(bf16[64,512]{1,0:T(8,128)(2,1)S(1)} %bitcast.67), channel_id=1, replica_groups=mesh['ep'=8,'tp'=4] {'tp'}, dimensions={1}, use_global_device_ids=true | all-gather | bytes 327680 | tf_op jit(solution)/shard_map/all_gather | solution.py:45
  43.2 3.0 %fusion.2 = f32[64,1024]{1,0:T(8,128)S(1)} fusion(bf16[64,2048]{1,0:T(8,128)(2,1)S(1)} %all_gather.3, bf16[1,2048,1024]{2,1,0:T(8,128)(2,1)} %param.9), kind=kOutput, calls=%fused_computation.4 | convolution fusion | flops 268435456 | bytes 4718592 | tf_op jit(solution)/shard_map/dot_general | solution.py:46
  46.2 0.0 copy-start.1
  46.2 6.3 %fusion.12 = bf16[4,64,512]{2,1,0:T(8,128)(2,1)} fusion(bf16[1024,4,512]{2,1,0:T(4,128)(2,1)} %reshape_squeeze.4, bf16[64,2048]{1,0:T(8,128)(2,1)S(1)} %all_gather.3, bf16[1,2048,1024]{2,1,0:T(8,128)(2,1)} %param.10, f32[64,1024]{1,0:T(8,128)S(1)} %fusion.2), kind=kOutput, calls=%fused_computation.10 | convolution fusion | flops 537395200 | bytes 9175040 | tf_op jit(solution)/shard_map/rf,fcd->crd/dot_general | solution.py:51
  52.6 0.0 reduce-scatter.4.cloned.1.call-update
  52.6 21.7 %reduce-scatter.4.cloned.1.call-done = bf16[1,64,512]{2,1,0:T(8,128)(2,1)} async-done(((bf16[4,64,512]{2,1,0:T(8,128)(2,1)}), bf16[1,64,512]{2,1,0:T(8,128)(2,1)}) %reduce-scatter.4.cloned.1.call-update) | async-done | bytes 65552
  74.3 4.6 %all-to-all-start = ((bf16[8,8,512]{2,1,0:T(8,128)(2,1)}), bf16[8,8,512]{2,1,0:T(8,128)(2,1)S(1)}, u32[]{:S(2)}, u32[]{:S(2)}) async-start(bf16[8,8,512]{2,1,0:T(8,128)(2,1)} %bitcast.69), calls=%async_computation | async-start | bytes 131072 | tf_op jit(solution)/shard_map/all_to_all | solution.py:59
  79.0 0.1 eq.27
  79.0 0.1 broadcast_in_dim.26
  79.1 5.8 %all-to-all-done = bf16[8,8,512]{2,1,0:T(8,128)(2,1)S(1)} async-done(((bf16[8,8,512]{2,1,0:T(8,128)(2,1)}), bf16[8,8,512]{2,1,0:T(8,128)(2,1)S(1)}, u32[]{:S(2)}, u32[]{:S(2)}) %all-to-all-start) | async-done | bytes 65568 | tf_op jit(solution)/shard_map/all_to_all | solution.py:59
  84.9 0.9 convolution_convert_fusion
  (24 shorter events, 0.1 us)
Async XLA Ops:
  6.5 1.1 %copy-start = (bf16[128,2048]{1,0:T(8,128)(2,1)S(1)}, bf16[128,2048]{1,0:T(8,128)(2,1)}, u32[]{:S(2)}) copy-start(bf16[128,2048]{1,0:T(8,128)(2,1)} %param.6) | copy-start | bytes 1572868
  6.5 67.8 %reduce-scatter.4.cloned.1.call-start = ((), (), s32[]{:S(2)}) async-start(), calls=%async_computation.2 | async-start | bytes 327680
  8.4 25.2 %collective-permute-start.6 = (bf16[1,8,512]{2,1,0:T(8,128)(2,1)S(1)}, bf16[1,8,512]{2,1,0:T(8,128)(2,1)S(1)}, u32[]{:S(2)}, u32[]{:S(2)}) collective-permute-start(bf16[1,8,512]{2,1,0:T(8,128)(2,1)S(1)} %get-tuple-element.7), channel_id=1, source_target_pairs={{0,28},{4,0},{8,4},{12,8},{16,12},{20,16},{24,20},{28,24},{1,29},{... | collective-permute-start | bytes 24584 | tf_op jit(solution)/shard_map/ppermute | solution.py:25
  13.0 20.6 %collective-permute-start.5 = (bf16[1,8,512]{2,1,0:T(8,128)(2,1)S(1)}, bf16[1,8,512]{2,1,0:T(8,128)(2,1)S(1)}, u32[]{:S(2)}, u32[]{:S(2)}) collective-permute-start(bf16[1,8,512]{2,1,0:T(8,128)(2,1)S(1)} %get-tuple-element.8), channel_id=1, source_target_pairs={{0,24},{4,28},{8,0},{12,4},{16,8},{20,12},{24,16},{28,20},{1,25},{... | collective-permute-start | bytes 24584 | tf_op jit(solution)/shard_map/ppermute | solution.py:25
  13.6 20.0 %collective-permute-start.4 = (bf16[1,8,512]{2,1,0:T(8,128)(2,1)S(1)}, bf16[1,8,512]{2,1,0:T(8,128)(2,1)S(1)}, u32[]{:S(2)}, u32[]{:S(2)}) collective-permute-start(bf16[1,8,512]{2,1,0:T(8,128)(2,1)S(1)} %get-tuple-element.9), channel_id=1, source_target_pairs={{0,20},{4,24},{8,28},{12,0},{16,4},{20,8},{24,12},{28,16},{1,21},{... | collective-permute-start | bytes 24584 | tf_op jit(solution)/shard_map/ppermute | solution.py:25
  13.6 20.0 %collective-permute-start.3 = (bf16[1,8,512]{2,1,0:T(8,128)(2,1)S(1)}, bf16[1,8,512]{2,1,0:T(8,128)(2,1)S(1)}, u32[]{:S(2)}, u32[]{:S(2)}) collective-permute-start(bf16[1,8,512]{2,1,0:T(8,128)(2,1)S(1)} %get-tuple-element.10), channel_id=1, source_target_pairs={{0,16},{4,20},{8,24},{12,28},{16,0},{20,4},{24,8},{28,12},{1,17},{... | collective-permute-start | bytes 24584 | tf_op jit(solution)/shard_map/ppermute | solution.py:25
  16.3 7.8 %collective-permute-start = (bf16[1,8,512]{2,1,0:T(8,128)(2,1)S(1)}, bf16[1,8,512]{2,1,0:T(8,128)(2,1)S(1)}, u32[]{:S(2)}, u32[]{:S(2)}) collective-permute-start(bf16[1,8,512]{2,1,0:T(8,128)(2,1)S(1)} %get-tuple-element.13), channel_id=1, source_target_pairs={{0,4},{4,8},{8,12},{12,16},{16,20},{20,24},{24,28},{28,0},{1,5},{5... | collective-permute-start | bytes 24584 | tf_op jit(solution)/shard_map/ppermute | solution.py:25
  24.2 5.4 %collective-permute-start.1 = (bf16[1,8,512]{2,1,0:T(8,128)(2,1)S(1)}, bf16[1,8,512]{2,1,0:T(8,128)(2,1)S(1)}, u32[]{:S(2)}, u32[]{:S(2)}) collective-permute-start(bf16[1,8,512]{2,1,0:T(8,128)(2,1)S(1)} %get-tuple-element.12), channel_id=1, source_target_pairs={{0,8},{4,12},{8,16},{12,20},{16,24},{20,28},{24,0},{28,4},{1,9},{5... | collective-permute-start | bytes 24584 | tf_op jit(solution)/shard_map/ppermute | solution.py:25
  29.6 4.0 %collective-permute-start.2 = (bf16[1,8,512]{2,1,0:T(8,128)(2,1)S(1)}, bf16[1,8,512]{2,1,0:T(8,128)(2,1)S(1)}, u32[]{:S(2)}, u32[]{:S(2)}) collective-permute-start(bf16[1,8,512]{2,1,0:T(8,128)(2,1)S(1)} %get-tuple-element.11), channel_id=1, source_target_pairs={{0,12},{4,16},{8,20},{12,24},{16,28},{20,0},{24,4},{28,8},{1,13},{... | collective-permute-start | bytes 24584 | tf_op jit(solution)/shard_map/ppermute | solution.py:25
  46.2 32.8 %copy-start.1 = (f32[1,8,8]{2,1,0:T(8,128)S(1)}, f32[1,8,8]{2,1,0:T(8,128)}, u32[]{:S(2)}) copy-start(f32[1,8,8]{2,1,0:T(8,128)} %param.8) | copy-start | bytes 772
  74.3 10.5 %all-to-all-start = ((bf16[8,8,512]{2,1,0:T(8,128)(2,1)}), bf16[8,8,512]{2,1,0:T(8,128)(2,1)S(1)}, u32[]{:S(2)}, u32[]{:S(2)}) async-start(bf16[8,8,512]{2,1,0:T(8,128)(2,1)} %bitcast.69), calls=%async_computation | async-start | bytes 131072 | tf_op jit(solution)/shard_map/all_to_all | solution.py:59
Sparse Core Ops, SparseCore 0:
  52.7 21.5 reduce-scatter.3
